TPU v7x, 32 devices: a whole 2x2x4 slice. The times are simulated.
32 devices in a mesh: sp: 16 (over z, y, x), tp: 2 (over core).
Axes of the slice: x: 2, y: 2, z: 4, core: 2. Of those that a mesh axis runs over, the one named last changes fastest.
Arguments:
- query_logits: bfloat16 [2048, 1024], P('sp', 'tp'), may hold values from -6 to 6
- value_rows: bfloat16 [2048, 1024], P('sp', 'tp'), may hold values from -6 to 6
- onward_forget_logits: bfloat16 [2048, 1024], P('sp', 'tp'), may hold values from -5.5 to 5.5
- reverse_forget_logits: bfloat16 [2048, 1024], P('sp', 'tp'), may hold values from -5.5 to 5.5
- output_gate_logits: bfloat16 [2048, 1024], P('sp', 'tp'), may hold values from -6 to 6
- onward_floor_gap: float32 [1024], P('tp'), may hold values from 0 to 0.12, as said below
- reverse_floor_gap: float32 [1024], P('tp'), may hold values from 0 to 0.12, as said below
- extra_log_decay: float32 [2048, 8], P('sp', 'tp'), may hold values from -2.1 to 0
- per_head_gain: float32 [128], replicated, may hold values from 0.1 to 1.9
- residual: bfloat16 [2048, 2048], P('sp', 'tp'), may hold values from -8 to 8
- output_matrix: bfloat16 [1024, 2048], P(None, 'tp'), may hold values from -0.375 to 0.375
- inner_norm_gain: float32 [2048], P('tp'), may hold values from 0.1 to 1.9
- inner_norm_bias: float32 [2048], P('tp'), may hold values from -1.5 to 1.5
- gate_matrix: bfloat16 [2048, 5632], P('sp', 'tp'), may hold values from -0.125 to 0.125
- up_matrix: bfloat16 [2048, 5632], P('sp', 'tp'), may hold values from -0.125 to 0.125
- down_matrix: bfloat16 [5632, 2048], P('tp', 'sp'), may hold values from -0.15625 to 0.15625
- closing_norm_gain: float32 [2048], P('tp'), may hold values from 0.1 to 1.9
- closing_norm_bias: float32 [2048], P('tp'), may hold values from -1.5 to 1.5
Outputs:
- layer_output: bfloat16 [2048, 2048], P('sp', 'tp')
Inputs may be any that keep to these rules, and one draw needn't show every extreme that they name: `onward_floor_gap`: positive. `reverse_floor_gap`: positive.
All inputs are finite; a program needn't handle non-finite values.
Results may differ from a plain program's by a relative error of at most 0.014.
Values may be sent and summed in bfloat16 or wider, within the bound.
A program may use at most 128 MiB of HBM per device.

v0:
```python
import math
import jax
import jax.numpy as jnp
from jax import lax
from jax.sharding import PartitionSpec as P

D = 2048
highest_precision = lax.Precision.HIGHEST
alpha_mix = 2.0**0.25
norm_eps = 1e-05
head_eps = 1e-06


def prefix(x, axis, join, neutral, backward):
    count = lax.axis_size(axis)
    place = lax.axis_index(axis)
    ahead = count - 1 - place if backward else place
    gathered = jax.tree.map(
        lambda a, kind: lax.all_gather(a.astype(kind), axis), x, (jnp.bfloat16, jnp.bfloat16)
    )
    state = jax.tree.map(lambda a, e: jnp.zeros_like(a) + jnp.asarray(e, a.dtype), x, neutral)

    def one(step, state):
        source = count - 1 - step if backward else step
        return join(
            state,
            jax.tree.map(
                lambda a, own: lax.dynamic_index_in_dim(a, source, 0, False).astype(own.dtype),
                gathered,
                x,
            ),
        )

    return lax.fori_loop(0, ahead, one, state)


def decay_factors(unscaled_input, lower_bound_gap, extra_decays):
    decay_factor = lower_bound_gap * jax.nn.sigmoid(-unscaled_input.astype(jnp.float32))
    return (jnp.log1p(-decay_factor) + extra_decays, decay_factor)


def local_pass(query, keys, values, log_decay):
    rows, head_count, model_width = query.shape
    span = math.gcd(rows, 128)
    count = rows // span
    triangle = jnp.tril(jnp.ones((span, span), jnp.float32))

    def blocks(array):
        return array.reshape(count, span, head_count, array.shape[2])

    def advance(carry, inputs):
        running_state, offset = carry
        query_block, key_block, value_tile, log_block = inputs
        running = jnp.cumsum(log_block, axis=0)
        final_index = running[-1]
        decayed_query = query_block * jnp.exp(running)
        key_inverse = key_block * jnp.exp(-running)
        key_stop = key_block * jnp.exp(final_index[None] - running)
        scores = (
            jnp.einsum("thk,shk->hts", decayed_query, key_inverse, precision=highest_precision)
            * triangle[None]
        )
        inner = jnp.einsum("hts,shv->thv", scores, value_tile, precision=highest_precision)
        carried_state = jnp.einsum(
            "nex,exl->nel", decayed_query, running_state, precision=highest_precision
        )
        query_start = decayed_query * jnp.exp(offset)[None]
        running_state = jnp.exp(final_index)[:, :, None] * running_state + jnp.einsum(
            "ojy,oje->jye", key_stop, value_tile, precision=highest_precision
        )
        return ((running_state, offset + final_index), (inner + carried_state, query_start))

    start = (
        jnp.zeros((head_count, model_width, values.shape[2]), jnp.float32),
        jnp.zeros((head_count, model_width), jnp.float32),
    )
    final, outputs = lax.scan(
        advance, start, (blocks(query), blocks(keys), blocks(values), blocks(log_decay))
    )
    result = outputs[0].reshape(rows, head_count, values.shape[2])
    query_start = outputs[1].reshape(rows, head_count, model_width)
    return (result, query_start, final[1], final[0])


def join(earlier, later):
    return (earlier[0] + later[0], jnp.exp(later[0])[:, :, None] * earlier[1] + later[1])


def row_norm(before, moments, gain, bias):
    mean = moments[0] / D
    spread = moments[1] / D - mean * mean
    return (before - mean[:, None]) * lax.rsqrt(spread + norm_eps)[:, None] * gain + bias


def shards(
    query_logits,
    value_rows,
    onward_forget_logits,
    reverse_forget_logits,
    output_gate_logits,
    onward_floor_gap,
    reverse_floor_gap,
    extra_log_decay,
    per_head_gain,
    residual,
    output_matrix,
    inner_norm_gain,
    inner_norm_bias,
    gate_matrix,
    up_matrix,
    down_matrix,
    closing_norm_gain,
    closing_norm_bias,
):
    gate_whole, up_whole, down_whole = (
        lax.all_gather(gate_matrix, "sp", axis=0, tiled=True),
        lax.all_gather(up_matrix, "sp", axis=0, tiled=True),
        lax.all_gather(down_matrix, "sp", axis=1, tiled=True),
    )
    rows = query_logits.shape[0]
    head_count = extra_log_decay.shape[1]
    model_width = query_logits.shape[1] // head_count
    shape_head = (rows, head_count, model_width)
    query = jax.nn.silu(query_logits.astype(jnp.float32)).reshape(shape_head)
    values = value_rows.astype(jnp.float32).reshape(shape_head)
    extra_decays = jnp.repeat(extra_log_decay, model_width, axis=1)
    onward_log_decay, onward_key_rows = decay_factors(
        onward_forget_logits, onward_floor_gap, extra_decays
    )
    reverse_log_decay, reverse_key_rows = decay_factors(
        reverse_forget_logits, reverse_floor_gap, extra_decays
    )
    empty_total = jnp.zeros((head_count, model_width), jnp.float32)
    empty_state = jnp.zeros((head_count, model_width, model_width), jnp.float32)
    upcoming_part, upcoming_begin, ahead_total, ahead_state = local_pass(
        query, onward_key_rows.reshape(shape_head), values, onward_log_decay.reshape(shape_head)
    )
    incoming_state = prefix(
        (ahead_total, ahead_state), "sp", join, (empty_total, empty_state), False
    )
    upcoming_part = upcoming_part + jnp.einsum(
        "nex,exl->nel", upcoming_begin, incoming_state[1], precision=highest_precision
    )
    preceding_part, preceding_begin, behind_total, behind_state = local_pass(
        jnp.flip(query, axis=0),
        jnp.flip(reverse_key_rows.reshape(shape_head), axis=0),
        jnp.flip(values, axis=0),
        jnp.flip(reverse_log_decay.reshape(shape_head), axis=0),
    )
    arriving_state = prefix(
        (behind_total, behind_state), "sp", join, (empty_total, empty_state), True
    )
    preceding_part = jnp.flip(
        preceding_part
        + jnp.einsum(
            "nex,exl->nel", preceding_begin, arriving_state[1], precision=highest_precision
        ),
        axis=0,
    )
    mixed = upcoming_part + preceding_part
    normed = (
        mixed * lax.rsqrt(jnp.mean(mixed * mixed, axis=2, keepdims=True) + head_eps) * per_head_gain
    )
    gated = (
        normed.reshape(rows, head_count * model_width)
        * jax.nn.silu(output_gate_logits.astype(jnp.float32))
    ).astype(jnp.bfloat16)
    mixer = jnp.dot(
        lax.all_gather(gated, "tp", axis=1, tiled=True),
        output_matrix,
        preferred_element_type=jnp.float32,
    )
    before_middle = alpha_mix * residual.astype(jnp.float32) + mixer
    moments = lax.psum(
        (jnp.sum(before_middle, axis=1), jnp.sum(before_middle * before_middle, axis=1)), "tp"
    )
    middle = row_norm(before_middle, moments, inner_norm_gain, inner_norm_bias).astype(jnp.bfloat16)
    whole = lax.all_gather(middle, "tp", axis=1, tiled=True)
    gate = jnp.dot(whole, gate_whole, preferred_element_type=jnp.float32)
    up = jnp.dot(whole, up_whole, preferred_element_type=jnp.float32)
    hidden = (jax.nn.silu(gate) * up).astype(jnp.bfloat16)
    partial_value = jnp.dot(hidden, down_whole, preferred_element_type=jnp.float32)
    feed = lax.psum_scatter(
        partial_value.astype(jnp.bfloat16), "tp", scatter_dimension=1, tiled=True
    ).astype(jnp.float32)
    before_final = alpha_mix * middle.astype(jnp.float32) + feed
    closing = lax.psum(
        (jnp.sum(before_final, axis=1), jnp.sum(before_final * before_final, axis=1)), "tp"
    )
    return row_norm(before_final, closing, closing_norm_gain, closing_norm_bias).astype(
        jnp.bfloat16
    )


def solution(mesh):
    placed = (
        P("sp", "tp"),
        P("sp", "tp"),
        P("sp", "tp"),
        P("sp", "tp"),
        P("sp", "tp"),
        P("tp"),
        P("tp"),
        P("sp", "tp"),
        P(),
        P("sp", "tp"),
        P(None, "tp"),
        P("tp"),
        P("tp"),
        P("sp", "tp"),
        P("sp", "tp"),
        P("tp", "sp"),
        P("tp"),
        P("tp"),
    )
    return jax.shard_map(
        shards, mesh=mesh, in_specs=placed, out_specs=P("sp", "tp"), check_vma=False
    )
```

profile of v0, /device:TPU:0, one launch (start us, length us, event | category | flops | bytes accessed | tf_op | source)
XLA Modules:
  0.0 643.3 jit_solution(78488061301699797)
XLA Ops:
  6.5 0.9 copy.35
  7.7 2.1 bitcast_add_fusion.1
  10.3 1.7 reshape.106
  12.1 0.8 squeeze.50
  12.8 1.0 convert_multiply_fusion.1
  13.8 0.8 squeeze.48
  14.8 2.4 exponential_multiply_fusion.3
  17.2 1.3 fusion.7
  18.6 2.0 fusion.6
  22.6 44.0 %all_gather.38 = bf16[16,4,128]{2,1,0:T(4,128)(2,1)} all-gather(bf16[1,4,128]{2,1,0:T(4,128)(2,1)S(1)} %slice.20), channel_id=1, replica_groups=mesh['sp'=16,'tp'=2] {'sp'}, dimensions={0}, use_global_device_ids=true | all-gather | bytes 17408 | tf_op jit(solution)/shard_map/all_gather | solution.py:19
  66.7 35.8 %all_gather.35 = bf16[16,4,128]{2,1,0:T(4,128)(2,1)S(1)} all-gather(bf16[1,4,128]{2,1,0:T(4,128)(2,1)S(1)} %slice.21), channel_id=1, replica_groups=mesh['sp'=16,'tp'=2] {'sp'}, dimensions={0}, use_global_device_ids=true | all-gather | bytes 17408 | tf_op jit(solution)/shard_map/all_gather | solution.py:19
  102.5 1.6 convolution_multiply_fusion.2
  107.2 26.5 %while.17 = (s32[]{:T(128)}, f32[4,128,128]{2,1,0:T(8,128)S(1)}, s32[]{:T(128)}, bf16[16,4,128]{2,1,0:T(4,128)(2,1)}, bf16[16,4,128,128]{3,2,1,0:T(8,128)(2,1)},...) while((s32[]{:T(128)}, f32[4,128,128]{2,1,0:T(8,128)S(1)}, s32[]{:T(128)}, bf16[16,4,128]{2,1,0:T(4,128)(2,1)}, ...), condition=%wide.region_5.6_spmd, body=%wide.region_4.5_spmd.sunk | while | flops 197126 | bytes 660627 | solution.py:34
  107.8 1.1 convert_add_fusion.6
  109.6 1.1 convert_add_fusion.6
  110.7 0.7 exponential_bitcast_fusion.5
  111.4 1.1 convert_add_fusion.6
  113.1 1.1 convert_add_fusion.6
  114.8 1.1 convert_add_fusion.6
  116.6 1.1 convert_add_fusion.6
  118.3 1.1 convert_add_fusion.6
  119.4 0.7 exponential_bitcast_fusion.5
  120.1 1.1 convert_add_fusion.6
  121.9 1.1 convert_add_fusion.6
  123.0 0.7 exponential_bitcast_fusion.5
  123.7 1.1 convert_add_fusion.6
  125.5 1.1 convert_add_fusion.6
  127.2 1.1 convert_add_fusion.6
  129.0 1.1 convert_add_fusion.6
  130.1 0.7 exponential_bitcast_fusion.5
  130.8 1.1 convert_add_fusion.6
  132.5 1.1 convert_add_fusion.6
  133.6 1.3 fusion.1
  134.9 1.9 rev.20
  136.9 7.2 %all-gather.14.cloned.1.call-done = bf16[64,128,128]{2,1,0:T(8,128)(2,1)} async-done(((bf16[4,128,128]{2,1,0:T(8,128)(2,1)}), bf16[64,128,128]{2,1,0:T(8,128)(2,1)}) %all-gather.14.cloned.1.call-update) | async-done | bytes 2097168 | tf_op jit(solution)/shard_map/all_gather | solution.py:19
  144.7 0.7 multiply_multiply_fusion
  145.7 2.0 all_gather.41
  148.3 2.5 all-reduce.1
  151.0 2.4 all_gather.42
  153.3 133.7 %all-gather.8.cloned.1.call-done = bf16[2048,2816]{1,0:T(8,128)(2,1)} async-done(((bf16[128,2816]{1,0:T(8,128)(2,1)}), bf16[2048,2816]{1,0:T(8,128)(2,1)}) %all-gather.8.cloned.1.call-update) | async-done | bytes 11534352 | tf_op jit(solution)/shard_map/all_gather | solution.py:116
  287.0 7.0 %fusion.40 = f32[128,2816]{1,0:T(8,128)} fusion(bf16[128,2048]{1,0:T(8,128)(2,1)S(1)} %all_gather.42, bf16[2048,2816]{1,0:T(8,128)(2,1)} %all-gather.8.cloned.1.call-done), kind=kOutput, calls=%fused_computation.91 | convolution fusion | flops 1476395008 | bytes 13500416 | tf_op jit(solution)/shard_map/dot_general | solution.py:179
  294.1 135.2 %all-gather.10.cloned.1.call-done = bf16[2048,2816]{1,0:T(8,128)(2,1)} async-done(((bf16[128,2816]{1,0:T(8,128)(2,1)}), bf16[2048,2816]{1,0:T(8,128)(2,1)}) %all-gather.10.cloned.1.call-update) | async-done | bytes 11534352 | tf_op jit(solution)/shard_map/all_gather | solution.py:117
  429.3 182.8 %all-gather.12.cloned.1.call-done = bf16[2816,2048]{1,0:T(8,128)(2,1)} async-done(((bf16[2816,128]{1,0:T(8,128)(2,1)}), bf16[2816,2048]{1,0:T(8,128)(2,1)}) %all-gather.12.cloned.1.call-update) | async-done | bytes 11534352 | tf_op jit(solution)/shard_map/all_gather | solution.py:118
  612.1 12.3 %convolution_convert_fusion = bf16[128,2048]{1,0:T(8,128)(2,1)} fusion(bf16[2816,2048]{1,0:T(8,128)(2,1)} %all-gather.12.cloned.1.call-done, bf16[128,2048]{1,0:T(8,128)(2,1)S(1)} %all_gather.42, bf16[2048,2816]{1,0:T(8,128)(2,1)} %all-gather.10.cloned.1.call-done, f32[128,2816]{1,0:T(8,128)} %fusion.40), kind=kOutput, calls=%fused_computation.6 | convolution fusion | flops 2955214848 | bytes 25559040 | tf_op jit(solution)/shard_map/dot_general | solution.py:182
  624.4 6.3 reduce-scatter.2.cloned.1.call-done
  630.7 1.3 fusion.8
  632.0 2.5 all-reduce
  634.5 1.9 add_convert_fusion
  (74 shorter events, 14.7 us)
Async XLA Ops:
  6.5 141.2 %copy-start = (bf16[1024,1024]{1,0:T(8,128)(2,1)S(1)}, bf16[1024,1024]{1,0:T(8,128)(2,1)}, u32[]{:S(2)}) copy-start(bf16[1024,1024]{1,0:T(8,128)(2,1)} %param.32) | copy-start | bytes 6291460
  6.5 100.6 %all-gather.16.cloned.1.call-start = ((), (), s32[]{:S(2)}) async-start(), calls=%async_computation.6 | async-start | bytes 2228224 | tf_op jit(solution)/shard_map/all_gather | solution.py:19
  9.8 4.8 copy-start.1
  9.9 2.1 copy-start.2
  18.5 125.5 %all-gather.14.cloned.1.call-start = ((), (), s32[]{:S(2)}) async-start(), calls=%async_computation.5 | async-start | bytes 2228224 | tf_op jit(solution)/shard_map/all_gather | solution.py:19
  20.6 266.4 %all-gather.8.cloned.1.call-start = ((), (), s32[]{:S(2)}) async-start(), calls=%async_computation.1 | async-start | bytes 12255232 | tf_op jit(solution)/shard_map/all_gather | solution.py:116
  21.4 407.9 %all-gather.10.cloned.1.call-start = ((), (), s32[]{:S(2)}) async-start(), calls=%async_computation.2 | async-start | bytes 12255232 | tf_op jit(solution)/shard_map/all_gather | solution.py:117
  22.0 590.1 %all-gather.12.cloned.1.call-start = ((), (), s32[]{:S(2)}) async-start(), calls=%async_computation.3 | async-start | bytes 12255232 | tf_op jit(solution)/shard_map/all_gather | solution.py:118
  22.5 608.2 %reduce-scatter.2.cloned.1.call-start = ((), (), s32[]{:S(2)}) async-start(), calls=%async_computation.4 | async-start | bytes 786432 | tf_op jit(solution)/shard_map/reduce_scatter | solution.py:183
  22.6 82.6 %copy-start.3 = (f32[128,4,128]{2,1,0:T(4,128)S(1)}, f32[128,4,128]{2,1,0:T(4,128)}, u32[]{:S(2)}) copy-start(f32[128,4,128]{2,1,0:T(4,128)} %get-tuple-element.229) | copy-start | bytes 786436
  144.1 1.5 copy-start.5
  144.1 3.7 copy-start.4
  145.6 5.2 copy-start.6
  145.6 5.2 copy-start.7
  294.1 340.4 %copy-start.8 = (f32[1024]{0:T(1024)S(1)}, f32[1024]{0:T(1024)}, u32[]{:S(2)}) copy-start(f32[1024]{0:T(1024)} %param.39) | copy-start | bytes 12292
  294.1 340.4 %copy-start.9 = (f32[1024]{0:T(1024)S(1)}, f32[1024]{0:T(1024)}, u32[]{:S(2)}) copy-start(f32[1024]{0:T(1024)} %param.38) | copy-start | bytes 12292
Sparse Core Ops, SparseCore 0:
  18.7 63.2 all-gather.15
  84.7 59.2 all-gather.13
  146.8 140.2 all-gather.7
  289.7 139.5 all-gather.9
  431.8 180.2 all-gather.11
  624.5 6.1 reduce-scatter.1
where the time goes:
time: 644 us; the launch traced here: 643 us
  waiting for transfers between devices  467 us (73%)
  blocking collectives  89.1 us (14%)
  other arithmetic  36 us (6%)
  matrix products  29.8 us (5%)
  between operations  13.7 us (2%)
  local copies, waits for them, and re-layouts  6.96 us (1%)
    all_gather x1, waiting for transfers between devices, shards(): lax.all_gather(down_matrix, 'sp', axis=1, tiled=True)  183 us
    all_gather x1, waiting for transfers between devices, shards(): lax.all_gather(up_matrix, 'sp', axis=0, tiled=True)  135 us
    all_gather x1, waiting for transfers between devices, shards(): lax.all_gather(gate_matrix, 'sp', axis=0, tiled=True)  134 us
    all_gather x2, blocking collectives, prefix(): lax.all_gather(a.astype(kind), axis)  79.8 us
    add x15, other arithmetic, join(): jnp.exp(later[0])[:, :, None] * earlier[1] + later[1]  16.1 us
  transfers between devices with their start and end apart: 6, of which 5 were waited for; matrix products, arithmetic and copies ran while one was open for 7% of the time, Pallas kernels for 0%

commit v1 on v0

--- a/solution.py
+++ b/solution.py
@@ -113,7 +113,9 @@
     closing_norm_bias,
 ):
     gate_whole, up_whole, down_whole = (
-        lax.all_gather(gate_matrix, "sp", axis=0, tiled=True),
+        jnp.concatenate(
+            lax.all_to_all(jnp.stack([gate_matrix] * lax.axis_size("sp")), "sp", 0, 0), axis=0
+        ),
         lax.all_gather(up_matrix, "sp", axis=0, tiled=True),
         lax.all_gather(down_matrix, "sp", axis=1, tiled=True),
     )

time: 644 us -> 706 us (1.096)
  blocking collectives: 89.1 us -> 345 us
  waiting for transfers between devices: 467 us -> 258 us
  starting transfers between devices: 0.2 us -> 8.55 us
    all_gather x2, blocking collectives: 79.8 us -> 335 us  [prefix(): lax.all_gather(a.astype(kind), axis)]
    all_gather x1 -> x0, waiting for transfers between devices: 134 us -> none  [shards(): lax.all_gather(gate_matrix, 'sp', axis=0, tiled=True)]
    all_gather x1, waiting for transfers between devices: 135 us -> 67.5 us  [shards(): lax.all_gather(up_matrix, 'sp', axis=0, tiled=True)]
    all_to_all x0 -> x1, starting transfers between devices: none -> 8.39 us  [shards(): lax.all_to_all(jnp.stack([gate_matrix] * lax.axis_size('sp')), 'sp', 0, 0)]
    all_gather x2, waiting for transfers between devices: 7.19 us -> 0.04 us  [prefix(): lax.all_gather(a.astype(kind), axis)]
  transfers between devices with their start and end apart: 6 -> 6, of which waited for: 5 -> 3; matrix products, arithmetic and copies ran while one was open for 7% -> 7% of each run, Pallas kernels for 0% -> 0%
where the time goes in v1:
time: 706 us; the launch traced here: 704 us
  blocking collectives  345 us (49%)
  waiting for transfers between devices  258 us (37%)
  other arithmetic  36 us (5%)
  matrix products  29.9 us (4%)
  between operations  13.4 us (2%)
  local copies, waits for them, and re-layouts  13.3 us (2%)
  starting transfers between devices  8.55 us (1%)
    all_gather x2, blocking collectives, prefix(): lax.all_gather(a.astype(kind), axis)  335 us
    all_gather x1, waiting for transfers between devices, shards(): lax.all_gather(down_matrix, 'sp', axis=1, tiled=True)  183 us
    all_gather x1, waiting for transfers between devices, shards(): lax.all_gather(up_matrix, 'sp', axis=0, tiled=True)  67.5 us
    add x15, other arithmetic, join(): jnp.exp(later[0])[:, :, None] * earlier[1] + later[1]  16.1 us
  transfers between devices with their start and end apart: 6, of which 3 were waited for; matrix products, arithmetic and copies ran while one was open for 7% of the time, Pallas kernels for 0%

profile of v1, /device:TPU:0, one launch (start us, length us, event | category | flops | bytes accessed | tf_op | source)
XLA Modules:
  0.0 704.4 jit_solution(14386993924600513553)
XLA Ops:
  6.5 0.9 copy.35
  7.7 2.0 bitcast_add_fusion.1
  10.2 1.7 reshape.111
  12.0 0.8 squeeze.50
  12.7 1.0 convert_multiply_fusion.1
  13.7 0.8 squeeze.48
  14.7 2.4 exponential_multiply_fusion.3
  17.1 1.3 fusion.7
  18.5 2.0 fusion.6
  21.2 6.4 stack.2
  27.6 8.4 %all-to-all-start = ((bf16[16,128,2816]{2,1,0:T(8,128)(2,1)}), bf16[16,128,2816]{2,1,0:T(8,128)(2,1)}, u32[]{:S(2)}, u32[]{:S(2)}) async-start(bf16[16,128,2816]{2,1,0:T(8,128)(2,1)} %stack.2), calls=%async_computation | async-start | bytes 23068672 | tf_op jit(solution)/shard_map/all_to_all | solution.py:117
  36.7 257.1 %all_gather.35 = bf16[16,4,128]{2,1,0:T(4,128)(2,1)} all-gather(bf16[1,4,128]{2,1,0:T(4,128)(2,1)S(1)} %slice.20), channel_id=1, replica_groups=mesh['sp'=16,'tp'=2] {'sp'}, dimensions={0}, use_global_device_ids=true | all-gather | bytes 17408 | tf_op jit(solution)/shard_map/all_gather | solution.py:19
  293.8 78.4 %all_gather.32 = bf16[16,4,128]{2,1,0:T(4,128)(2,1)S(1)} all-gather(bf16[1,4,128]{2,1,0:T(4,128)(2,1)S(1)} %slice.21), channel_id=1, replica_groups=mesh['sp'=16,'tp'=2] {'sp'}, dimensions={0}, use_global_device_ids=true | all-gather | bytes 17408 | tf_op jit(solution)/shard_map/all_gather | solution.py:19
  372.2 1.6 convolution_multiply_fusion.2
  376.9 26.5 %while.17 = (s32[]{:T(128)}, f32[4,128,128]{2,1,0:T(8,128)S(1)}, s32[]{:T(128)}, bf16[16,4,128]{2,1,0:T(4,128)(2,1)}, bf16[16,4,128,128]{3,2,1,0:T(8,128)(2,1)},...) while((s32[]{:T(128)}, f32[4,128,128]{2,1,0:T(8,128)S(1)}, s32[]{:T(128)}, bf16[16,4,128]{2,1,0:T(4,128)(2,1)}, ...), condition=%wide.region_5.6_spmd, body=%wide.region_4.5_spmd.sunk | while | flops 197126 | bytes 660627 | solution.py:34
  377.6 1.1 convert_add_fusion.6
  379.3 1.1 convert_add_fusion.6
  381.1 1.1 convert_add_fusion.6
  382.9 1.1 convert_add_fusion.6
  384.6 1.1 convert_add_fusion.6
  386.4 1.1 convert_add_fusion.6
  387.5 0.7 exponential_bitcast_fusion.5
  388.2 1.1 convert_add_fusion.6
  389.9 1.1 convert_add_fusion.6
  391.1 0.7 exponential_bitcast_fusion.5
  391.7 1.1 convert_add_fusion.6
  392.9 0.7 exponential_bitcast_fusion.5
  393.5 1.1 convert_add_fusion.6
  395.3 1.1 convert_add_fusion.6
  397.0 1.1 convert_add_fusion.6
  398.1 0.7 exponential_bitcast_fusion.5
  398.8 1.1 convert_add_fusion.6
  400.6 1.1 convert_add_fusion.6
  402.3 1.1 convert_add_fusion.6
  403.4 1.3 fusion.1
  404.7 1.9 rev.20
  407.4 0.7 multiply_multiply_fusion
  408.4 2.0 all_gather.38
  411.0 2.5 all-reduce.1
  413.6 2.4 all_gather.39
  416.0 7.1 %fusion.40 = f32[128,2816]{1,0:T(8,128)} fusion(bf16[128,2048]{1,0:T(8,128)(2,1)S(1)} %all_gather.39, bf16[2048,2816]{1,0:T(8,128)(2,1)} %bitcast.15), kind=kOutput, calls=%fused_computation.91 | convolution fusion | flops 1476395008 | bytes 13500416 | tf_op jit(solution)/shard_map/dot_general | solution.py:181
  423.1 67.5 %all-gather.7.cloned.1.call-done = bf16[2048,2816]{1,0:T(8,128)(2,1)} async-done(((bf16[128,2816]{1,0:T(8,128)(2,1)}), bf16[2048,2816]{1,0:T(8,128)(2,1)}) %all-gather.7.cloned.1.call-update) | async-done | bytes 11534352 | tf_op jit(solution)/shard_map/all_gather | solution.py:119
  490.6 182.8 %all-gather.9.cloned.1.call-done = bf16[2816,2048]{1,0:T(8,128)(2,1)} async-done(((bf16[2816,128]{1,0:T(8,128)(2,1)}), bf16[2816,2048]{1,0:T(8,128)(2,1)}) %all-gather.9.cloned.1.call-update) | async-done | bytes 11534352 | tf_op jit(solution)/shard_map/all_gather | solution.py:120
  673.4 12.5 %convolution_convert_fusion = bf16[128,2048]{1,0:T(8,128)(2,1)} fusion(bf16[2816,2048]{1,0:T(8,128)(2,1)} %all-gather.9.cloned.1.call-done, bf16[128,2048]{1,0:T(8,128)(2,1)S(1)} %all_gather.39, bf16[2048,2816]{1,0:T(8,128)(2,1)} %all-gather.7.cloned.1.call-done, f32[128,2816]{1,0:T(8,128)} %fusion.40), kind=kOutput, calls=%fused_computation.6 | convolution fusion | flops 2955214848 | bytes 25559040 | tf_op jit(solution)/shard_map/dot_general | solution.py:184
  685.9 6.3 reduce-scatter.2.cloned.1.call-done
  692.1 1.3 fusion.8
  693.4 2.5 all-reduce
  695.9 1.9 add_convert_fusion
  (74 shorter events, 14.1 us)
Async XLA Ops:
  6.5 403.9 %copy-start = (bf16[1024,1024]{1,0:T(8,128)(2,1)S(1)}, bf16[1024,1024]{1,0:T(8,128)(2,1)}, u32[]{:S(2)}) copy-start(bf16[1024,1024]{1,0:T(8,128)(2,1)} %param.32) | copy-start | bytes 6291460
  6.5 370.3 %all-gather.13.cloned.1.call-start = ((), (), s32[]{:S(2)}) async-start(), calls=%async_computation.6 | async-start | bytes 2228224 | tf_op jit(solution)/shard_map/all_gather | solution.py:19
  9.8 4.8 copy-start.2
  18.4 388.3 %all-gather.11.cloned.1.call-start = ((), (), s32[]{:S(2)}) async-start(), calls=%async_computation.5 | async-start | bytes 2228224 | tf_op jit(solution)/shard_map/all_gather | solution.py:19
  20.5 470.1 %all-gather.7.cloned.1.call-start = ((), (), s32[]{:S(2)}) async-start(), calls=%async_computation.2 | async-start | bytes 12255232 | tf_op jit(solution)/shard_map/all_gather | solution.py:119
  27.6 388.4 %all-to-all-start = ((bf16[16,128,2816]{2,1,0:T(8,128)(2,1)}), bf16[16,128,2816]{2,1,0:T(8,128)(2,1)}, u32[]{:S(2)}, u32[]{:S(2)}) async-start(bf16[16,128,2816]{2,1,0:T(8,128)(2,1)} %stack.2), calls=%async_computation | async-start | bytes 23068672 | tf_op jit(solution)/shard_map/all_to_all | solution.py:117
  36.0 637.4 %all-gather.9.cloned.1.call-start = ((), (), s32[]{:S(2)}) async-start(), calls=%async_computation.3 | async-start | bytes 12255232 | tf_op jit(solution)/shard_map/all_gather | solution.py:120
  36.6 655.5 %reduce-scatter.2.cloned.1.call-start = ((), (), s32[]{:S(2)}) async-start(), calls=%async_computation.4 | async-start | bytes 786432 | tf_op jit(solution)/shard_map/reduce_scatter | solution.py:185
  36.7 338.2 %copy-start.3 = (f32[128,4,128]{2,1,0:T(4,128)S(1)}, f32[128,4,128]{2,1,0:T(4,128)}, u32[]{:S(2)}) copy-start(f32[128,4,128]{2,1,0:T(4,128)} %get-tuple-element.229) | copy-start | bytes 786436
  406.7 1.5 copy-start.5
  406.7 3.7 copy-start.4
  408.3 5.2 copy-start.6
  408.3 5.2 copy-start.7
  423.1 272.8 %copy-start.8 = (f32[1024]{0:T(1024)S(1)}, f32[1024]{0:T(1024)}, u32[]{:S(2)}) copy-start(f32[1024]{0:T(1024)} %param.39) | copy-start | bytes 12292
  423.1 272.8 %copy-start.9 = (f32[1024]{0:T(1024)S(1)}, f32[1024]{0:T(1024)}, u32[]{:S(2)}) copy-start(f32[1024]{0:T(1024)} %param.38) | copy-start | bytes 12292
  673.4 24.4 %copy-start.1 = (bf16[1024,1024]{1,0:T(8,128)(2,1)S(1)}, bf16[1024,1024]{1,0:T(8,128)(2,1)}, u32[]{:S(2)}) copy-start(bf16[1024,1024]{1,0:T(8,128)(2,1)} %param.32) | copy-start | bytes 6291460
Sparse Core Ops, SparseCore 0:
  18.5 244.7 all-gather.12
  266.1 81.4 all-gather.10
  350.4 140.1 all-gather.6
  493.1 180.2 all-gather.8
  686.0 6.0 reduce-scatter.1
